TPU v7x, 32 devices: a whole 2x2x4 slice. The times are simulated.
32 devices in a mesh: sp: 16 (over z, x, core), tp: 2 (over y).
Axes of the slice: x: 2, y: 2, z: 4, core: 2. Of those that a mesh axis runs over, the one named last changes fastest.
Arguments:
- skip_connection_stream: bfloat16 [12288, 2048], P('sp'), may hold values from -6 to 6
- probing_vectors: bfloat16 [12288, 512], P('sp', 'tp'), may hold values from -6 to 6
- addressing_vectors: bfloat16 [12288, 512], P('sp', 'tp'), may hold values from -6 to 6
- mapped_payloads: bfloat16 [12288, 1024], P('sp', 'tp'), may hold values from -6 to 6
- emission_switch: bfloat16 [12288, 1024], P('sp', 'tp'), may hold values from -6 to 6
- lapse_preactivation: bfloat16 [12288, 512], P('sp', 'tp')
- lapse_shift_entries: float32 [512], P('tp')
- surplus_attenuation_terms: float32 [12288], P('sp'), may hold values from -0.7 to 0
- passage_label_per_token: int32 [12288], P('sp'), may hold values from 0 to 3, never falling along the last dimension, each value on 1 to 6144 neighbouring positions
- attention_group_rescaler: float32 [128], replicated, may hold values from 0.1 to 1.9
- emission_projector: bfloat16 [1024, 2048], P('tp'), may hold values from -0.1875 to 0.1875
- perceptron_rescaler: float32 [2048], replicated, may hold values from 0.1 to 1.9
- switching_projector: bfloat16 [2048, 5632], P('sp', 'tp'), may hold values from -0.125 to 0.125
- widening_projector: bfloat16 [2048, 5632], P('sp', 'tp'), may hold values from -0.125 to 0.125
- shrinking_projector: bfloat16 [5632, 2048], P('tp', 'sp'), may hold values from -0.078125 to 0.078125
Outputs:
- layer_out: bfloat16 [12288, 2048], P(('sp', 'tp'))
Inputs may be any that keep to these rules, and one draw needn't show every extreme that they name: `passage_label_per_token`: document numbers never fall along the sequence; a document holds at most 6144 positions.
All inputs are finite; a program needn't handle non-finite values.
Results may differ from a plain program's by a relative error of at most 0.014.
Values may be sent and summed in bfloat16 or wider, within the bound.
A program may use at most 128 MiB of HBM per device.

v0:
```python
import jax
import jax.numpy as jnp
from jax import lax
from jax.sharding import PartitionSpec as P

DK = 64
DV = 128
BLOCK = 64
eps = 1e-06
sharpness_factor = 16.0


def entering(shard, axis, join, neutral):
    place = lax.axis_index(axis)
    gathered = jax.tree.map(
        lambda a, kind: lax.all_gather(a.astype(kind), axis),
        shard,
        jax.tree.map(lambda a: jnp.bfloat16 if a.dtype == jnp.float32 else a.dtype, shard),
    )
    state = jax.tree.map(lambda a, e: jnp.zeros_like(a) + jnp.asarray(e, a.dtype), shard, neutral)

    def one(turn, state):
        return join(
            state,
            jax.tree.map(
                lambda a, own: lax.dynamic_index_in_dim(a, turn, 0, False).astype(own.dtype),
                gathered,
                shard,
            ),
        )

    return lax.fori_loop(0, place, one, state)


def head_split(array, heads):
    return array.reshape(array.shape[0], heads, -1).transpose(1, 0, 2)


def block_pass(
    query_head_rows,
    key_heads,
    value_heads,
    decay_heads,
    documents,
    recurrent_state,
    last_doc,
    offset,
    span,
):
    heads, length, _ = query_head_rows.shape
    blocks = length // span
    middle = span // 2

    def to_blocks(array):
        return array.reshape(heads, blocks, span, array.shape[-1]).transpose(1, 0, 2, 3)

    lower = jnp.tril(jnp.ones((span, span), dtype=bool))

    def step(carry, inputs):
        recurrent_state, last_doc, offset = carry
        query_block, key_blk, value_block, piece_attenuation, doc_blk = inputs
        cumulative_decay = jnp.cumsum(piece_attenuation, axis=1)
        previous_valid = (doc_blk == last_doc).astype(jnp.float32)
        cross_block_output = (
            jnp.einsum("gfl,glm->gfm", query_block * jnp.exp(cumulative_decay), recurrent_state)
            * previous_valid[None, :, None]
        )
        centre = cumulative_decay[:, middle : middle + 1, :]
        query_scaled = query_block * jnp.exp(cumulative_decay - centre)
        key_scaled = key_blk * jnp.exp(centre - cumulative_decay)
        same = (doc_blk[:, None] == doc_blk[None, :]) & lower
        raw_scores = jnp.einsum("hik,hjk->hij", query_scaled, key_scaled)
        scores = jnp.where(same[None, :, :], raw_scores, 0.0)
        result = cross_block_output + jnp.einsum("hij,hjv->hiv", scores, value_block)
        final_memory_summary = cumulative_decay[:, -1, :]
        last_valid = (doc_blk[-1] == last_doc).astype(jnp.float32)
        tail_ok = (doc_blk == doc_blk[-1]).astype(jnp.float32)
        decayed_keys = (
            key_blk
            * jnp.exp(final_memory_summary[:, None, :] - cumulative_decay)
            * tail_ok[None, :, None]
        )
        recurrent_state = recurrent_state * jnp.exp(final_memory_summary)[
            :, :, None
        ] * last_valid + jnp.einsum("wrz,wrs->wzs", decayed_keys, value_block)
        return (
            (recurrent_state, doc_blk[-1], offset + final_memory_summary),
            (result, cumulative_decay + offset[:, None, :]),
        )

    carry, outputs = lax.scan(
        step,
        (recurrent_state, last_doc, offset),
        (
            to_blocks(query_head_rows),
            to_blocks(key_heads),
            to_blocks(value_heads),
            to_blocks(decay_heads),
            documents.reshape(blocks, span),
        ),
    )
    result, running_state = outputs
    result = result.transpose(1, 0, 2, 3).reshape(heads, length, -1)
    running_state = running_state.transpose(1, 0, 2, 3).reshape(heads, length, -1)
    return (carry[0], carry[2], result, running_state)


def join_spans(earlier, later):
    linked = ((earlier[3] == later[2]) | (earlier[3] < 0.0) | (later[2] < 0.0)).astype(jnp.float32)
    decay_total = earlier[0] * later[0] * linked
    state_total = earlier[1] * (later[0] * linked)[:, :, None] + later[1]
    first_doc = jnp.where(earlier[2] < 0.0, later[2], earlier[2])
    final_doc = jnp.where(later[3] < 0.0, earlier[3], later[3])
    return (decay_total, state_total, first_doc, final_doc)


def rms_rows(rows, gain):
    wide = rows.astype(jnp.float32)
    return (wide * lax.rsqrt(jnp.mean(wide * wide, axis=-1, keepdims=True) + eps) * gain).astype(
        jnp.bfloat16
    )


def per_device(
    skip_connection_stream,
    probing_vectors,
    addressing_vectors,
    mapped_payloads,
    emission_switch,
    lapse_preactivation,
    lapse_shift_entries,
    surplus_attenuation_terms,
    passage_label_per_token,
    attention_group_rescaler,
    emission_projector,
    perceptron_rescaler,
    switching_projector,
    widening_projector,
    shrinking_projector,
):
    rows_here = skip_connection_stream.shape[0]
    heads_here = probing_vectors.shape[1] // DK
    keeping_exponent = (
        jax.nn.log_sigmoid(lapse_preactivation.astype(jnp.float32) + lapse_shift_entries[None, :])
        / sharpness_factor
        + surplus_attenuation_terms[:, None]
    )
    query_head_rows = head_split(probing_vectors.astype(jnp.float32) * DK ** (-0.5), heads_here)
    key_heads = head_split(addressing_vectors.astype(jnp.float32), heads_here)
    value_heads = head_split(mapped_payloads.astype(jnp.float32), heads_here)
    decay_heads = head_split(keeping_exponent, heads_here)
    zero_state = jnp.zeros((heads_here, DK, DV), jnp.float32)
    state_local, total_log, local_out, running_state = block_pass(
        query_head_rows,
        key_heads,
        value_heads,
        decay_heads,
        passage_label_per_token,
        zero_state,
        passage_label_per_token[0],
        jnp.zeros((heads_here, DK), jnp.float32),
        BLOCK,
    )
    unbroken = (passage_label_per_token[0] == passage_label_per_token[-1]).astype(jnp.float32)
    summary = (
        jnp.exp(total_log) * unbroken,
        state_local,
        passage_label_per_token[0].astype(jnp.float32),
        passage_label_per_token[-1].astype(jnp.float32),
    )
    identity = (
        jnp.ones_like(total_log),
        jnp.zeros_like(state_local),
        jnp.full((), -1.0, jnp.float32),
        jnp.full((), -1.0, jnp.float32),
    )
    carried_state = entering(summary, "sp", join_spans, identity)
    reaches = (passage_label_per_token.astype(jnp.float32) == carried_state[3]).astype(jnp.float32)
    incoming = (
        jnp.einsum("qlj,qjf->qlf", query_head_rows * jnp.exp(running_state), carried_state[1])
        * reaches[None, :, None]
    )
    attn = local_out + incoming
    normed_attn = (
        attn
        * lax.rsqrt(jnp.mean(attn * attn, axis=-1, keepdims=True) + eps)
        * attention_group_rescaler
    )
    flat = normed_attn.transpose(1, 0, 2).reshape(rows_here, heads_here * DV)
    gated = (flat * jax.nn.silu(emission_switch.astype(jnp.float32))).astype(jnp.bfloat16)
    share_rows = rows_here // lax.axis_size("tp")
    own_start = lax.axis_index("tp") * share_rows
    mixed = lax.psum(
        jnp.dot(gated, emission_projector, preferred_element_type=jnp.float32).astype(jnp.bfloat16),
        "tp",
    ).astype(jnp.float32)
    first_all = (skip_connection_stream.astype(jnp.float32) + mixed).astype(jnp.bfloat16)
    normed = rms_rows(first_all, perceptron_rescaler)
    first_own = lax.dynamic_slice_in_dim(first_all, own_start, share_rows, 0)
    gate = jnp.dot(
        normed,
        lax.all_gather(switching_projector, "sp", axis=0, tiled=True),
        preferred_element_type=jnp.float32,
    )
    upper = jnp.dot(
        normed,
        lax.all_gather(widening_projector, "sp", axis=0, tiled=True),
        preferred_element_type=jnp.float32,
    )
    hidden = (jax.nn.silu(gate) * upper).astype(jnp.bfloat16)
    terms = jnp.dot(
        hidden,
        lax.all_gather(shrinking_projector, "sp", axis=1, tiled=True),
        preferred_element_type=jnp.float32,
    )
    ffn_out = lax.psum_scatter(
        terms.astype(jnp.bfloat16), "tp", scatter_dimension=0, tiled=True
    ).astype(jnp.float32)
    return (first_own.astype(jnp.float32) + 0.5 * ffn_out).astype(jnp.bfloat16)


def solution(mesh):
    placed = (
        P("sp", None),
        P("sp", "tp"),
        P("sp", "tp"),
        P("sp", "tp"),
        P("sp", "tp"),
        P("sp", "tp"),
        P("tp"),
        P("sp"),
        P("sp"),
        P(),
        P("tp", None),
        P(),
        P("sp", "tp"),
        P("sp", "tp"),
        P("tp", "sp"),
    )
    return jax.shard_map(
        per_device, mesh=mesh, in_specs=placed, out_specs=P(("sp", "tp"), None), check_vma=False
    )
```

profile of v0, /device:TPU:0, one launch (start us, length us, event | category | flops | bytes accessed | tf_op | source)
XLA Modules:
  0.0 747.7 jit_solution(6886762841094768849)
XLA Ops:
  10.6 1.8 reshape.144
  14.6 2.7 reshape.150
  19.1 1.8 reshape.137
  23.6 117.2 %while.35 = (s32[]{:T(128)}, f32[4,64,128]{2,1,0:T(8,128)S(1)}, s32[]{:T(128)}, f32[4,64]{1,0:T(4,128)S(1)}, f32[12,4,64,128]{3,2,0,1:T(8,128)}, /*index=5*/f32[...) while((s32[]{:T(128)}, f32[4,64,128]{2,1,0:T(8,128)S(1)}, ...), condition=%wide.region_2.3_spmd.clone, body=%wide.region_0.2_spmd.clone.sunk | while | flops 16118533 | bytes 2851019 | solution.py:91
  27.4 1.8 fusion.85
  37.2 1.8 fusion.85
  46.9 1.8 fusion.85
  56.7 1.8 fusion.85
  66.5 1.8 fusion.85
  76.2 1.8 fusion.85
  95.8 1.8 fusion.85
  105.5 1.8 fusion.85
  125.1 1.8 fusion.85
  134.8 1.8 fusion.85
  144.9 35.1 %all-reduce.2 = (bf16[16]{0:T(256)(128)(2,1)S(1)}, bf16[16]{0:T(256)(128)(2,1)S(1)}) all-reduce(bf16[16]{0:T(256)(128)(2,1)S(1)} %dynamic-update-slice, bf16[16]{0:T(256)(128)(2,1)S(1)} %dynamic-update-slice.1), channel_id=1, replica_groups=mesh['sp'=16,'tp'=2] {'sp'}, use_global_device_ids=true, to_apply=%add | all-reduce | flops 32 | bytes 128
  181.2 2.8 exponential_bitcast_fusion
  184.0 3.0 copy.57
  186.9 2.7 exp.47
  189.6 3.1 copy.58
  192.8 17.1 %all-gather.2 = bf16[16,4,64]{2,1,0:T(4,128)(2,1)S(1)} all-gather(bf16[1,4,64]{2,1,0:T(4,128)(2,1)S(1)} %fusion.58), channel_id=2, replica_groups=mesh['sp'=16,'tp'=2] {'sp'}, dimensions={0}, use_global_device_ids=true | all-gather | bytes 8704 | tf_op jit(solution)/shard_map/all_gather | solution.py:16
  210.0 2.1 multiply_reduce_fusion
  213.5 3.0 copy.59
  216.6 4.9 convolution_convert_fusion
  223.6 154.7 %all-reduce.5.cloned.1.call-done = bf16[768,2048]{1,0:T(8,128)(2,1)} async-done(((bf16[768,2048]{1,0:T(8,128)(2,1)}), bf16[768,2048]{1,0:T(8,128)(2,1)}) %all-reduce.5.cloned.1.call-update) | async-done | bytes 3145744 | tf_op jit(solution)/shard_map/psum | solution.py:193
  378.3 6.0 fusion.36
  384.3 90.3 %all-gather.8.cloned.1.call-done = bf16[2048,2816]{1,0:T(8,128)(2,1)} async-done(((bf16[128,2816]{1,0:T(8,128)(2,1)}), bf16[2048,2816]{1,0:T(8,128)(2,1)}) %all-gather.8.cloned.1.call-update) | async-done | bytes 11534352 | tf_op jit(solution)/shard_map/all_gather | solution.py:202
  474.6 15.9 %fusion.49 = f32[768,2816]{1,0:T(8,128)} fusion(bf16[2048,2816]{1,0:T(8,128)(2,1)} %all-gather.8.cloned.1.call-done, bf16[768,2048]{1,0:T(8,128)(2,1)} %get-tuple-element.262, f32[2048]{0:T(1024)S(1)} %copy-done.9, f32[768]{0:T(1024)S(1)} %add_rsqrt_fusion.1), kind=kOutput, calls=%fused_computation.73 | convolution fusion | flops 8864661504 | bytes 23342080 | tf_op jit(solution)/shard_map/dot_general | solution.py:200
  490.6 78.5 %all-gather.10.cloned.1.call-done = bf16[2048,2816]{1,0:T(8,128)(2,1)} async-done(((bf16[128,2816]{1,0:T(8,128)(2,1)}), bf16[2048,2816]{1,0:T(8,128)(2,1)}) %all-gather.10.cloned.1.call-update) | async-done | bytes 11534352 | tf_op jit(solution)/shard_map/all_gather | solution.py:207
  569.0 97.2 %all-gather.12.cloned.1.call-done = bf16[2816,2048]{1,0:T(8,128)(2,1)} async-done(((bf16[2816,128]{1,0:T(8,128)(2,1)}), bf16[2816,2048]{1,0:T(8,128)(2,1)}) %all-gather.12.cloned.1.call-update) | async-done | bytes 11534352 | tf_op jit(solution)/shard_map/all_gather | solution.py:213
  666.2 29.2 %fusion.41 = bf16[768,2048]{1,0:T(8,128)(2,1)} fusion(bf16[2816,2048]{1,0:T(8,128)(2,1)} %all-gather.12.cloned.1.call-done, f32[768,2816]{1,0:T(8,128)} %fusion.49, bf16[2048,2816]{1,0:T(8,128)(2,1)} %all-gather.10.cloned.1.call-done, bf16[768,2048]{1,0:T(8,128)(2,1)} %get-tuple-element.262, f32[2048]{0:T(1024)S(1)} %copy-done.9, f32[768]{0:T(1024)S(1)} %add_rsqrt_fusion.1), kind=kOutput, calls=%fused_computation.57 | convolution fusion | flops 17737580544 | bytes 38022144 | tf_op jit(solution)/shard_map/dot_general | solution.py:211
  695.4 41.7 %reduce-scatter.2.cloned.1.call-done = bf16[384,2048]{1,0:T(8,128)(2,1)} async-done(((bf16[768,2048]{1,0:T(8,128)(2,1)}), bf16[384,2048]{1,0:T(8,128)(2,1)}) %reduce-scatter.2.cloned.1.call-update) | async-done | bytes 1572880 | tf_op jit(solution)/shard_map/reduce_scatter | solution.py:216
  737.1 3.7 add_convert_fusion.1
  (244 shorter events, 100.5 us)
Async XLA Ops:
  6.5 210.0 %copy-start = (bf16[512,2048]{1,0:T(8,128)(2,1)S(1)}, bf16[512,2048]{1,0:T(8,128)(2,1)}, u32[]{:S(2)}) copy-start(bf16[512,2048]{1,0:T(8,128)(2,1)} %param.29) | copy-start | bytes 6291460
  6.5 203.4 %all-gather.14.cloned.1.call-start = ((), (), s32[]{:S(2)}) async-start(), calls=%async_computation.6 | async-start | bytes 1114112 | tf_op jit(solution)/shard_map/all_gather | solution.py:16
  10.6 6.7 copy-start.2
  12.4 6.1 copy-start.5
  12.5 6.1 copy-start.6
  23.6 119.2 %copy-start.10 = (u32[32]{0:T(128)S(1)}, u32[32]{0:T(128)}, u32[]{:S(2)}) copy-start(u32[32]{0:T(128)} %constant.98) | copy-start | bytes 388
  141.5 236.9 %all-reduce.5.cloned.1.call-start = ((), (), s32[]{:S(2)}) async-start(), calls=%async_computation.1 | async-start | bytes 6291456 | tf_op jit(solution)/shard_map/psum | solution.py:193
  189.6 20.3 %copy-start.4 = (s32[768]{0:T(1024)S(1)}, s32[768]{0:T(1024)}, u32[]{:S(2)}) copy-start(s32[768]{0:T(1024)} %param.27) | copy-start | bytes 9220
  189.6 20.4 %copy-start.3 = (f32[768,256]{0,1:T(8,128)S(1)}, f32[768,256]{0,1:T(8,128)}, u32[]{:S(2)}) copy-start(f32[768,256]{0,1:T(8,128)} %copy-done.2) | copy-start | bytes 2359300
  209.9 2.2 copy-start.7
  212.2 4.4 copy-start.8
  221.5 253.2 %all-gather.8.cloned.1.call-start = ((), (), s32[]{:S(2)}) async-start(), calls=%async_computation.2 | async-start | bytes 12255232 | tf_op jit(solution)/shard_map/all_gather | solution.py:202
  222.2 346.8 %all-gather.10.cloned.1.call-start = ((), (), s32[]{:S(2)}) async-start(), calls=%async_computation.3 | async-start | bytes 12255232 | tf_op jit(solution)/shard_map/all_gather | solution.py:207
  222.8 443.4 %all-gather.12.cloned.1.call-start = ((), (), s32[]{:S(2)}) async-start(), calls=%async_computation.4 | async-start | bytes 12255232 | tf_op jit(solution)/shard_map/all_gather | solution.py:213
  223.4 251.3 %copy-start.9 = (f32[2048]{0:T(1024)S(1)}, f32[2048]{0:T(1024)}, u32[]{:S(2)}) copy-start(f32[2048]{0:T(1024)} %param.30) | copy-start | bytes 24580
  223.4 513.7 %reduce-scatter.2.cloned.1.call-start = ((), (), s32[]{:S(2)}) async-start(), calls=%async_computation.5 | async-start | bytes 4718592 | tf_op jit(solution)/shard_map/reduce_scatter | solution.py:216
  695.4 45.4 %copy-start.1 = (bf16[512,2048]{1,0:T(8,128)(2,1)S(1)}, bf16[512,2048]{1,0:T(8,128)(2,1)}, u32[]{:S(2)}) copy-start(bf16[512,2048]{1,0:T(8,128)(2,1)} %param.29) | copy-start | bytes 6291460
Sparse Core Ops, SparseCore 0:
  141.6 40.5 all-gather.13
  221.6 156.6 all-reduce.4
  380.6 93.9 all-gather.7
  476.8 92.2 all-gather.9
  571.0 95.1 all-gather.11
  695.5 41.5 reduce-scatter.1
where the time goes:
time: 752 us; the launch traced here: 748 us
  waiting for transfers between devices  464 us (62%)
  matrix products  89.2 us (12%)
  local copies, waits for them, and re-layouts  78.8 us (10%)
  blocking collectives  52.2 us (7%)
  other arithmetic  31.1 us (4%)
  between operations  16.8 us (2%)
  loops' own time  15 us (2%)
    psum x1, waiting for transfers between devices, per_device(): lax.psum(jnp.dot(gated, emission_projector, preferred_element_type=jnp.fl...  155 us
    all_gather x1, waiting for transfers between devices, per_device(): lax.all_gather(shrinking_projector, 'sp', axis=1, tiled=True)  97.2 us
    all_gather x1, waiting for transfers between devices, per_device(): lax.all_gather(switching_projector, 'sp', axis=0, tiled=True)  90.3 us
    all_gather x1, waiting for transfers between devices, per_device(): lax.all_gather(widening_projector, 'sp', axis=0, tiled=True)  78.5 us
    reduce_scatter x1, waiting for transfers between devices, per_device(): lax.psum_scatter(terms.astype(jnp.bfloat16), 'tp', scatter_dimension=0, t...  41.7 us
    dynamic_slice x60, local copies, waits for them, and re-layouts, block_pass(): lax.scan(step, (recurrent_state, last_doc, offset), (to_blocks(query_head...  40.2 us
    unnamed x1, blocking collectives  35.1 us
    dot_general x1, matrix products, per_device(): jnp.dot(hidden, lax.all_gather(shrinking_projector, 'sp', axis=1, tiled=T...  29.2 us
  transfers between devices with their start and end apart: 6, of which 5 were waited for; matrix products, arithmetic and copies ran while one was open for 5% of the time, Pallas kernels for 0%

commit v1 on v0

--- a/solution.py
+++ b/solution.py
@@ -210,7 +210,7 @@
     hidden = (jax.nn.silu(gate) * upper).astype(jnp.bfloat16)
     terms = jnp.dot(
         hidden,
-        lax.all_gather(shrinking_projector, "sp", axis=1, tiled=True),
+        jnp.concatenate(jax.lax.all_gather(shrinking_projector, "sp"), 1),
         preferred_element_type=jnp.float32,
     )
     ffn_out = lax.psum_scatter(

time: 752 us -> 754 us (level)
  waiting for transfers between devices: 464 us -> 446 us
  local copies, waits for them, and re-layouts: 78.8 us -> 94 us
    reshape x0 -> x1, local copies, waits for them, and re-layouts: none -> 15.2 us  [per_device(): jnp.concatenate(jax.lax.all_gather(shrinking_projector, 'sp'), 1)]
    all_gather x1, waiting for transfers between devices: 90.3 us -> 79.2 us  [per_device(): lax.all_gather(switching_projector, 'sp', axis=0, tiled=True)]
  transfers between devices with their start and end apart: 6 -> 6, of which waited for: 5 -> 5; matrix products, arithmetic and copies ran while one was open for 5% -> 7% of each run, Pallas kernels for 0% -> 0%
where the time goes in v1:
time: 754 us; the launch traced here: 750 us
  waiting for transfers between devices  446 us (59%)
  matrix products  94.1 us (12%)
  local copies, waits for them, and re-layouts  94 us (12%)
  blocking collectives  52.2 us (7%)
  other arithmetic  31.1 us (4%)
  between operations  16.8 us (2%)
  loops' own time  15 us (2%)
    psum x1, waiting for transfers between devices, per_device(): lax.psum(jnp.dot(gated, emission_projector, preferred_element_type=jnp.fl...  155 us
    all_gather x1, waiting for transfers between devices, per_device(): jax.lax.all_gather(shrinking_projector, 'sp')  90.3 us
    all_gather x1, waiting for transfers between devices, per_device(): lax.all_gather(switching_projector, 'sp', axis=0, tiled=True)  79.2 us
    all_gather x1, waiting for transfers between devices, per_device(): lax.all_gather(widening_projector, 'sp', axis=0, tiled=True)  78.6 us
    reduce_scatter x1, waiting for transfers between devices, per_device(): lax.psum_scatter(terms.astype(jnp.bfloat16), 'tp', scatter_dimension=0, t...  41.8 us
    dynamic_slice x60, local copies, waits for them, and re-layouts, block_pass(): lax.scan(step, (recurrent_state, last_doc, offset), (to_blocks(query_head...  40.2 us
    unnamed x1, blocking collectives  35.1 us
    dot_general x1, matrix products, per_device(): jnp.dot(hidden, jnp.concatenate(jax.lax.all_gather(shrinking_projector, '...  34.2 us
  transfers between devices with their start and end apart: 6, of which 5 were waited for; matrix products, arithmetic and copies ran while one was open for 7% of the time, Pallas kernels for 0%

profile of v1, /device:TPU:0, one launch (start us, length us, event | category | flops | bytes accessed | tf_op | source)
XLA Modules:
  0.0 750.0 jit_solution(3865380202980922380)
XLA Ops:
  10.6 1.8 reshape.150
  14.6 2.7 reshape.158
  19.1 1.8 reshape.143
  23.6 117.2 %while.35 = (s32[]{:T(128)}, f32[4,64,128]{2,1,0:T(8,128)S(1)}, s32[]{:T(128)}, f32[4,64]{1,0:T(4,128)S(1)}, f32[12,4,64,128]{3,2,0,1:T(8,128)}, /*index=5*/f32[...) while((s32[]{:T(128)}, f32[4,64,128]{2,1,0:T(8,128)S(1)}, ...), condition=%wide.region_2.3_spmd.clone, body=%wide.region_0.2_spmd.clone.sunk | while | flops 16118533 | bytes 2851019 | solution.py:91
  27.4 1.8 fusion.82
  46.9 1.8 fusion.82
  56.7 1.8 fusion.82
  66.5 1.8 fusion.82
  76.2 1.8 fusion.82
  95.8 1.8 fusion.82
  105.5 1.8 fusion.82
  125.1 1.8 fusion.82
  134.8 1.8 fusion.82
  144.9 35.1 %all-reduce.2 = (bf16[16]{0:T(256)(128)(2,1)S(1)}, bf16[16]{0:T(256)(128)(2,1)S(1)}) all-reduce(bf16[16]{0:T(256)(128)(2,1)S(1)} %dynamic-update-slice, bf16[16]{0:T(256)(128)(2,1)S(1)} %dynamic-update-slice.1), channel_id=1, replica_groups=mesh['sp'=16,'tp'=2] {'sp'}, use_global_device_ids=true, to_apply=%add | all-reduce | flops 32 | bytes 128
  181.2 2.8 exponential_bitcast_fusion
  184.0 3.0 copy.58
  186.9 2.7 exp.47
  189.6 3.1 copy.59
  192.8 17.1 %all-gather.3 = bf16[16,4,64]{2,1,0:T(4,128)(2,1)S(1)} all-gather(bf16[1,4,64]{2,1,0:T(4,128)(2,1)S(1)} %fusion.55), channel_id=2, replica_groups=mesh['sp'=16,'tp'=2] {'sp'}, dimensions={0}, use_global_device_ids=true | all-gather | bytes 8704 | tf_op jit(solution)/shard_map/all_gather | solution.py:16
  210.0 2.1 multiply_reduce_fusion
  213.5 3.0 copy.60
  216.6 4.9 convolution_convert_fusion
  223.6 154.7 %all-reduce.5.cloned.1.call-done = bf16[768,2048]{1,0:T(8,128)(2,1)} async-done(((bf16[768,2048]{1,0:T(8,128)(2,1)}), bf16[768,2048]{1,0:T(8,128)(2,1)}) %all-reduce.5.cloned.1.call-update) | async-done | bytes 3145744 | tf_op jit(solution)/shard_map/psum | solution.py:193
  378.3 6.0 fusion.36
  384.3 90.3 %all-gather.15.cloned.1.call-done = bf16[45056,128]{1,0:T(8,128)(2,1)} async-done(((bf16[2816,128]{1,0:T(8,128)(2,1)}), bf16[45056,128]{1,0:T(8,128)(2,1)}) %all-gather.15.cloned.1.call-update) | async-done | bytes 11534352 | tf_op jit(solution)/shard_map/all_gather | solution.py:213
  474.6 15.2 %copy.61 = bf16[2816,16,128]{0,2,1:T(8,128)(2,1)} copy(bf16[2816,16,128]{2,0,1:T(8,128)(2,1)} %bitcast.140) | data formatting | bytes 23068672 | tf_op jit(solution)/shard_map/reshape | solution.py:213
  489.9 79.2 %all-gather.9.cloned.1.call-done = bf16[2048,2816]{1,0:T(8,128)(2,1)} async-done(((bf16[128,2816]{1,0:T(8,128)(2,1)}), bf16[2048,2816]{1,0:T(8,128)(2,1)}) %all-gather.9.cloned.1.call-update) | async-done | bytes 11534352 | tf_op jit(solution)/shard_map/all_gather | solution.py:202
  569.0 15.8 %fusion.46 = f32[768,2816]{1,0:T(8,128)} fusion(bf16[2048,2816]{1,0:T(8,128)(2,1)} %all-gather.9.cloned.1.call-done, bf16[768,2048]{1,0:T(8,128)(2,1)} %get-tuple-element.262, f32[2048]{0:T(1024)S(1)} %copy-done.9, f32[768]{0:T(1024)S(1)} %add_rsqrt_fusion.1), kind=kOutput, calls=%fused_computation.71 | convolution fusion | flops 8864661504 | bytes 23342080 | tf_op jit(solution)/shard_map/dot_general | solution.py:200
  584.9 78.6 %all-gather.11.cloned.1.call-done = bf16[2048,2816]{1,0:T(8,128)(2,1)} async-done(((bf16[128,2816]{1,0:T(8,128)(2,1)}), bf16[2048,2816]{1,0:T(8,128)(2,1)}) %all-gather.11.cloned.1.call-update) | async-done | bytes 11534352 | tf_op jit(solution)/shard_map/all_gather | solution.py:207
  663.4 34.2 %convolution_convert_fusion.1 = bf16[768,2048]{1,0:T(8,128)(2,1)} fusion(bf16[2816,2048]{0,1:T(8,128)(2,1)} %bitcast.141, f32[768,2816]{1,0:T(8,128)} %fusion.46, bf16[2048,2816]{1,0:T(8,128)(2,1)} %all-gather.11.cloned.1.call-done, bf16[768,2048]{1,0:T(8,128)(2,1)} %get-tuple-element.262, f32[2048]{0:T(1024)S(1)} %copy-done.9, f32[768]{0:T(1024)S(1)} %add_rsqrt_fusion.1), kind=kOutput, calls=%fused_computation.56 | convolution fusion | flops 17737580544 | bytes 38022144 | tf_op jit(solution)/shard_map/dot_general | solution.py:211
  697.6 41.8 %reduce-scatter.2.cloned.1.call-done = bf16[384,2048]{1,0:T(8,128)(2,1)} async-done(((bf16[768,2048]{1,0:T(8,128)(2,1)}), bf16[384,2048]{1,0:T(8,128)(2,1)}) %reduce-scatter.2.cloned.1.call-update) | async-done | bytes 1572880 | tf_op jit(solution)/shard_map/reduce_scatter | solution.py:216
  739.5 3.7 add_convert_fusion.1
  (245 shorter events, 102.3 us)
Async XLA Ops:
  6.5 210.0 %copy-start = (bf16[512,2048]{1,0:T(8,128)(2,1)S(1)}, bf16[512,2048]{1,0:T(8,128)(2,1)}, u32[]{:S(2)}) copy-start(bf16[512,2048]{1,0:T(8,128)(2,1)} %param.29) | copy-start | bytes 6291460
  6.5 203.4 %all-gather.13.cloned.1.call-start = ((), (), s32[]{:S(2)}) async-start(), calls=%async_computation.5 | async-start | bytes 1114112 | tf_op jit(solution)/shard_map/all_gather | solution.py:16
  10.6 6.7 copy-start.2
  12.4 6.1 copy-start.5
  12.5 6.1 copy-start.6
  23.6 119.2 %copy-start.10 = (u32[32]{0:T(128)S(1)}, u32[32]{0:T(128)}, u32[]{:S(2)}) copy-start(u32[32]{0:T(128)} %constant.98) | copy-start | bytes 388
  141.5 236.9 %all-reduce.5.cloned.1.call-start = ((), (), s32[]{:S(2)}) async-start(), calls=%async_computation.1 | async-start | bytes 6291456 | tf_op jit(solution)/shard_map/psum | solution.py:193
  189.6 20.3 %copy-start.4 = (s32[768]{0:T(1024)S(1)}, s32[768]{0:T(1024)}, u32[]{:S(2)}) copy-start(s32[768]{0:T(1024)} %param.27) | copy-start | bytes 9220
  189.6 20.4 %copy-start.3 = (f32[768,256]{0,1:T(8,128)S(1)}, f32[768,256]{0,1:T(8,128)}, u32[]{:S(2)}) copy-start(f32[768,256]{0,1:T(8,128)} %copy-done.2) | copy-start | bytes 2359300
  209.9 2.2 copy-start.7
  212.2 4.4 copy-start.8
  221.5 253.2 %all-gather.15.cloned.1.call-start = ((), (), s32[]{:S(2)}) async-start(), calls=%async_computation.6 | async-start | bytes 12255232 | tf_op jit(solution)/shard_map/all_gather | solution.py:213
  222.2 346.8 %all-gather.9.cloned.1.call-start = ((), (), s32[]{:S(2)}) async-start(), calls=%async_computation.2 | async-start | bytes 12255232 | tf_op jit(solution)/shard_map/all_gather | solution.py:202
  222.8 440.6 %all-gather.11.cloned.1.call-start = ((), (), s32[]{:S(2)}) async-start(), calls=%async_computation.3 | async-start | bytes 12255232 | tf_op jit(solution)/shard_map/all_gather | solution.py:207
  223.4 516.1 %reduce-scatter.2.cloned.1.call-start = ((), (), s32[]{:S(2)}) async-start(), calls=%async_computation.4 | async-start | bytes 4718592 | tf_op jit(solution)/shard_map/reduce_scatter | solution.py:216
  474.6 94.4 %copy-start.9 = (f32[2048]{0:T(1024)S(1)}, f32[2048]{0:T(1024)}, u32[]{:S(2)}) copy-start(f32[2048]{0:T(1024)} %param.30) | copy-start | bytes 24580
  697.6 45.5 %copy-start.1 = (bf16[512,2048]{1,0:T(8,128)(2,1)S(1)}, bf16[512,2048]{1,0:T(8,128)(2,1)}, u32[]{:S(2)}) copy-start(bf16[512,2048]{1,0:T(8,128)(2,1)} %param.29) | copy-start | bytes 6291460
Sparse Core Ops, SparseCore 0:
  141.6 40.5 all-gather.12
  221.6 156.6 all-reduce.4
  380.6 93.9 all-gather.14
  476.8 92.2 all-gather.8
  571.2 92.2 all-gather.10
  697.7 41.6 reduce-scatter.1
